TPU v7x, 512 devices: a whole 4x4x16 slice. The times are simulated.
512 devices in a mesh: fs: 64 (over z, y), tp: 8 (over x, core).
Axes of the slice: x: 4, y: 4, z: 16, core: 2. Of those that a mesh axis runs over, the one named last changes fastest.
Arguments:
- tokens: bfloat16 [16384, 2048], P('fs', 'tp'), may hold values from -16 to 16, as said below
- mix_gain: bfloat16 [2048], P('tp'), may hold values from 0.099609375 to 1.8984375
- query_weight: bfloat16 [2048, 512], P('fs', 'tp'), may hold values from -0.125 to 0.125
- key_weight: bfloat16 [2048, 512], P('fs', 'tp'), may hold values from -0.125 to 0.125
- value_weight: bfloat16 [2048, 1024], P('fs', 'tp'), may hold values from -0.125 to 0.125
- output_gate_weight: bfloat16 [2048, 1024], P('fs', 'tp'), may hold values from -0.125 to 0.125
- out_weight: bfloat16 [1024, 2048], P('tp', 'fs'), may hold values from -0.1875 to 0.1875
- head_rates: float32 [8], P('tp'), may hold values from 0 to 1, as said below
- block_scale: float32 [128], P('fs'), may hold values from 0.5 to 2
- ffn_gain: bfloat16 [2048], P('tp'), may hold values from 0.099609375 to 1.8984375
- ff_gate: bfloat16 [2048, 5632], P('fs', 'tp'), may hold values from -0.125 to 0.125
- ff_up: bfloat16 [2048, 5632], P('fs', 'tp'), may hold values from -0.125 to 0.125
- ff_down: bfloat16 [5632, 2048], P('tp', 'fs'), may hold values from -0.078125 to 0.078125
- final_gain: bfloat16 [2048], P('tp'), may hold values from 0.099609375 to 1.8984375
Outputs:
- layer_out: bfloat16 [16384, 2048], P('fs', 'tp')
Inputs may be any that keep to these rules, and one draw needn't show every extreme that they name: `tokens`: column blocks of the activations have different scales. `head_rates`: positive rates.
All inputs are finite; a program needn't handle non-finite values.
Results may differ from a plain program's by a relative error of at most 0.014.
Values may be sent and summed in bfloat16 or wider, within the bound.
A program may use at most 64 MiB of HBM per device.

v0:
```python
import jax
import jax.numpy as jnp
from jax import lax
from jax.sharding import Mesh
from jax.sharding import PartitionSpec as P

D = 2048
DK = 64
DV = 128
BLK = 128
SEQ_LEN = 256
FS = ("fs_0", "fs_1")
EPS = 1e-06
THETA = 10000.0


def gather_turned(arrays, axis, dims):
    turned = [jnp.moveaxis(a, dim, 0) for a, dim in zip(arrays, dims)]
    both = jnp.concatenate([t.reshape(len(t), -1) for t in turned], axis=1)
    filled, at, outs = (lax.all_gather(both, axis, axis=0, tiled=True), 0, [])
    for t, dim in zip(turned, dims):
        share = filled[:, at : at + t[0].size].reshape(-1, *t.shape[1:])
        outs.append(jnp.moveaxis(share, 0, dim))
        at += t[0].size
    return tuple(outs)


def sent_together(arrays, axis, dim, along):
    widths = [a.shape[along] for a in arrays]
    both = jnp.concatenate(arrays, axis=along)
    filled = lax.all_gather(both, axis, axis=dim, tiled=True)
    return tuple(jnp.split(filled, [sum(widths[:k]) for k in range(1, len(widths))], axis=along))


def laid_out(tiles, dim):
    lengths = list(tiles.shape[1:])
    lengths[dim] *= tiles.shape[0]
    return jnp.moveaxis(tiles, 0, dim).reshape(lengths)


def copy_for_each(shard, axis):
    size = lax.axis_size(axis)
    return lax.all_to_all(
        jnp.broadcast_to(shard[None], (size, *shard.shape)), axis, 0, 0, tiled=True
    )


def gather_directly(shard, axis, dim):
    return laid_out(copy_for_each(shard, axis), dim)


def gathered_by_axis(shard, axes, dim):
    filled = shard
    for number in range(len(axes) - 1, -1, -1):
        filled = lax.all_gather(filled, axes[number], axis=dim, tiled=True)
    return filled


def in_blocks(shard, dim, size):
    lengths = shard.shape
    tiles = shard.reshape(*lengths[:dim], size, lengths[dim] // size, *lengths[dim + 1 :])
    return jnp.moveaxis(tiles, dim, 0)


def sent_and_summed(shard, axis, dim):
    size = lax.axis_size(axis)
    tiles = lax.all_to_all(in_blocks(shard, dim, size), axis, 0, 0, tiled=True)
    return jnp.sum(tiles.astype(jnp.float32), axis=0)


def of_everyone(shard, axis):
    return copy_for_each(shard, axis).sum(axis=0)


def rms_norm(values, gain):
    scale = lax.rsqrt(jnp.mean(values * values, axis=-1, keepdims=True) + EPS)
    return values * scale * gain.astype(jnp.float32)


def rotate(values, positions):
    half = values.shape[-1] // 2
    inverse = THETA ** (-jnp.arange(half, dtype=jnp.float32) / half)
    angle = positions.astype(jnp.float32)[:, None] * inverse
    cosine = jnp.cos(angle)[:, None, :]
    sine = jnp.sin(angle)[:, None, :]
    first = values[..., :half]
    second = values[..., half:]
    return jnp.concatenate(
        [first * cosine - second * sine, second * cosine + first * sine], axis=-1
    )


def retain(query, key, value, rates, scales):
    rows, heads_here, width_k = query.shape
    width_v = value.shape[-1]
    nblk = rows // BLK
    hi = lax.Precision.HIGHEST
    qblk = query.astype(jnp.float32).reshape(nblk, BLK, heads_here, width_k)
    kblk = key.astype(jnp.float32).reshape(nblk, BLK, heads_here, width_k)
    vblk = value.astype(jnp.float32).reshape(nblk, BLK, heads_here, width_v)
    logdec = -rates[None, :] * scales[:, None]
    steps = jnp.arange(BLK, dtype=jnp.float32)
    offset = steps[:, None] - steps[None, :]
    causal = offset >= 0
    inside = jnp.where(
        causal[None, None],
        jnp.exp(logdec[:, :, None, None] * jnp.where(causal, offset, 0.0)[None, None]),
        0.0,
    )
    scores = jnp.einsum("nchd,nmhd->nhcm", qblk, kblk, precision=hi) * inside
    inner = jnp.einsum("nhcm,nmhe->nche", scores, vblk, precision=hi)
    zeta = jnp.exp(logdec[:, :, None] * (BLK - 1.0 - steps)[None, None, :])
    kv_block = jnp.einsum(
        "nchd,nche->nhde", kblk * jnp.transpose(zeta, (0, 2, 1))[..., None], vblk, precision=hi
    )
    hold = jnp.exp(logdec * BLK)
    per_seq = SEQ_LEN // BLK
    fresh = (jnp.arange(nblk, dtype=jnp.int32) % per_seq == 0).astype(jnp.float32)

    def advance(state, inputs):
        kv_now, hold_now, fresh_now = inputs
        before = state * (1.0 - fresh_now)
        return (before * hold_now[:, None, None] + kv_now, before)

    start = jnp.zeros((heads_here, width_k, width_v), jnp.float32)
    _, before = lax.scan(advance, start, (kv_block, hold, fresh))
    xi = jnp.exp(logdec[:, :, None] * (steps + 1.0)[None, None, :])
    cross = jnp.einsum(
        "nchd,nhde->nche", qblk * jnp.transpose(xi, (0, 2, 1))[..., None], before, precision=hi
    )
    total = inner + cross
    total = total * lax.rsqrt(jnp.mean(total * total, axis=-1, keepdims=True) + EPS)
    return total.reshape(rows, heads_here * width_v)


def body(
    tokens,
    mix_gain,
    query_weight,
    key_weight,
    value_weight,
    output_gate_weight,
    out_weight,
    head_rates,
    block_scale,
    ffn_gain,
    ff_gate,
    ff_up,
    ff_down,
    final_gain,
):
    rows = tokens.shape[0]
    heads_here = head_rates.shape[0]
    groups = lax.axis_size("tp")
    positions = jnp.arange(rows, dtype=jnp.int32) % SEQ_LEN
    whole, gain_whole = gather_turned((tokens, mix_gain), "tp", (1, 0))
    normed = rms_norm(whole.astype(jnp.float32), gain_whole).astype(jnp.bfloat16)
    collected = sent_together(
        (query_weight, key_weight, value_weight, output_gate_weight), FS, 0, 1
    )
    qproj, kproj, vproj, gproj = tuple(
        (jnp.dot(normed, weight, preferred_element_type=jnp.float32) for weight in collected)
    )
    query = rotate(qproj.reshape(rows, heads_here, DK), positions).astype(jnp.bfloat16)
    key = (rotate(kproj.reshape(rows, heads_here, DK), positions) * DK ** (-0.5)).astype(
        jnp.bfloat16
    )
    value = vproj.astype(jnp.bfloat16).reshape(rows, heads_here, DV)
    normret = retain(query, key, value, head_rates, block_scale)
    gated = (normret * jax.nn.silu(gproj)).astype(jnp.bfloat16)
    all_heads = gather_directly(gated, "tp", 1)
    head_rows = gathered_by_axis(out_weight, FS, 1)
    feature_block = lax.all_to_all(head_rows, "tp", split_axis=1, concat_axis=0, tiled=True)
    width = all_heads.shape[1] // groups
    left = all_heads.reshape(rows, groups, width)
    right = feature_block.reshape(groups, width, feature_block.shape[1])
    partial_sums = jnp.einsum(
        "rng,nge->nre", left, right, preferred_element_type=jnp.float32
    ).astype(jnp.bfloat16)
    mix = jnp.sum(partial_sums.astype(jnp.float32), axis=0)
    resid = (tokens.astype(jnp.float32) + mix).astype(jnp.bfloat16)
    whole2, gain2 = gather_turned((resid, ffn_gain), "tp", (1, 0))
    normed2 = rms_norm(whole2.astype(jnp.float32), gain2).astype(jnp.bfloat16)
    gate_rows, up_rows = sent_together((ff_gate, ff_up), FS, 0, 1)
    gate_part = jnp.dot(normed2, gate_rows, preferred_element_type=jnp.float32)
    up_part = jnp.dot(normed2, up_rows, preferred_element_type=jnp.float32)
    hidden = (jax.nn.silu(gate_part) * up_part).astype(jnp.bfloat16)
    down_terms = jnp.dot(
        hidden, gathered_by_axis(ff_down, FS, 1), preferred_element_type=jnp.float32
    )
    ffn = sent_and_summed(down_terms.astype(jnp.bfloat16), "tp", 1)
    total = resid.astype(jnp.float32) + ffn
    squares = of_everyone(jnp.sum(total * total, axis=-1, keepdims=True), "tp")
    scale = lax.rsqrt(squares / D + EPS)
    return (total * scale * final_gain.astype(jnp.float32)).astype(jnp.bfloat16)


def solution(mesh):
    finer = Mesh(mesh.devices.reshape(16, 4, mesh.shape["tp"]), ("fs_0", "fs_1", "tp"))
    return jax.shard_map(
        body,
        mesh=finer,
        in_specs=(
            P(FS, "tp"),
            P("tp"),
            P(FS, "tp"),
            P(FS, "tp"),
            P(FS, "tp"),
            P(FS, "tp"),
            P("tp", FS),
            P("tp"),
            P(FS),
            P("tp"),
            P(FS, "tp"),
            P(FS, "tp"),
            P("tp", FS),
            P("tp"),
        ),
        out_specs=P(FS, "tp"),
        check_vma=False,
    )
```

profile of v0, /device:TPU:1, one launch (start us, length us, event | category | flops | bytes accessed | tf_op | source)
XLA Modules:
  0.0 515.7 jit_solution(17452584656318330392)
XLA Ops:
  7.2 1.6 pad_maximum_fusion
  8.9 1.4 pad_maximum_fusion.3
  10.3 10.6 %all_gather.26 = bf16[128,128]{0,1:T(8,128)(2,1)S(1)} all-gather(bf16[128,32]{0,1:T(8,128)(2,1)} %param.22), channel_id=1, replica_groups=mesh['fs_0'=16,'fs_1'=4,'tp'=8] {'fs_1'}, dimensions={1}, use_global_device_ids=true | all-gather | bytes 40960 | tf_op jit(solution)/shard_map/all_gather | solution.py:55
  20.9 31.9 %all_gather.27 = bf16[128,2048]{0,1:T(8,128)(2,1)S(1)} all-gather(bf16[128,128]{0,1:T(8,128)(2,1)S(1)} %all_gather.26), channel_id=1, replica_groups=mesh['fs_0'=16,'fs_1'=4,'tp'=8] {'fs_0'}, dimensions={1}, use_global_device_ids=true | all-gather | bytes 557056 | tf_op jit(solution)/shard_map/all_gather | solution.py:55
  53.8 14.1 %all-to-all-start.1 = ((bf16[128,8,256]{2,0,1:T(8,128)(2,1)}), bf16[128,8,256]{2,0,1:T(8,128)(2,1)S(1)}, u32[]{:S(2)}, u32[]{:S(2)}) async-start(bf16[128,8,256]{2,0,1:T(8,128)(2,1)} %copy.31), calls=%async_computation.1 | async-start | bytes 1048576 | tf_op jit(solution)/shard_map/all_to_all | solution.py:173
  68.9 1.6 fusion.4
  71.2 109.0 %all-gather.8.cloned.1.call-done = bf16[2048,384]{1,0:T(8,128)(2,1)} async-done(((bf16[32,384]{1,0:T(8,128)(2,1)}), bf16[2048,384]{1,0:T(8,128)(2,1)}) %all-gather.8.cloned.1.call-update) | async-done | bytes 1572880 | tf_op jit(solution)/shard_map/all_gather | solution.py:31
  180.3 2.0 convolution_bitcast_fusion
  182.3 1.6 convolution_bitcast_fusion.1
  184.2 1.5 convolution_convert_fusion.2
  185.9 5.0 while.13
  192.1 1.6 fusion.35
  194.6 15.1 %all-to-all-start = ((bf16[8,256,128]{2,1,0:T(8,128)(2,1)}), bf16[8,256,128]{2,1,0:T(8,128)(2,1)S(1)}, u32[]{:S(2)}, u32[]{:S(2)}) async-start(bf16[8,256,128]{2,1,0:T(8,128)(2,1)} %broadcast_in_dim.29), calls=%async_computation | async-start | bytes 1048576 | tf_op jit(solution)/shard_map/all_to_all | solution.py:43
  209.7 9.3 %all-to-all-done = bf16[8,256,128]{2,1,0:T(8,128)(2,1)S(1)} async-done(((bf16[8,256,128]{2,1,0:T(8,128)(2,1)}), bf16[8,256,128]{2,1,0:T(8,128)(2,1)S(1)}, u32[]{:S(2)}, u32[]{:S(2)}) %all-to-all-start) | async-done | bytes 524320 | tf_op jit(solution)/shard_map/all_to_all | solution.py:43
  221.1 10.0 %all_gather.30 = bf16[704,128]{0,1:T(8,128)(2,1)} all-gather(bf16[704,32]{0,1:T(8,128)(2,1)S(1)} %copy-done.5), channel_id=1, replica_groups=mesh['fs_0'=16,'fs_1'=4,'tp'=8] {'fs_1'}, dimensions={1}, use_global_device_ids=true | all-gather | bytes 225280 | tf_op jit(solution)/shard_map/all_gather | solution.py:55
  231.1 15.0 %all-gather.10.cloned.1.call-done = bf16[2048,257]{0,1:T(8,128)(2,1)} async-done(((bf16[256,257]{0,1:T(8,128)(2,1)}), bf16[2048,257]{0,1:T(8,128)(2,1)}) %all-gather.10.cloned.1.call-update) | async-done | bytes 1052688 | tf_op jit(solution)/shard_map/all_gather | solution.py:20
  246.0 1.5 fusion.7
  248.3 142.7 %all-gather.12.cloned.1.call-done = bf16[2048,1408]{1,0:T(8,128)(2,1)} async-done(((bf16[32,1408]{1,0:T(8,128)(2,1)}), bf16[2048,1408]{1,0:T(8,128)(2,1)}) %all-gather.12.cloned.1.call-update) | async-done | bytes 5767184 | tf_op jit(solution)/shard_map/all_gather | solution.py:31
  391.0 3.7 fusion.2
  394.7 68.0 %all-gather.14.cloned.1.call-done = bf16[704,2048]{0,1:T(8,128)(2,1)} async-done(((bf16[704,128]{0,1:T(8,128)(2,1)}), bf16[704,2048]{0,1:T(8,128)(2,1)}) %all-gather.14.cloned.1.call-update) | async-done | bytes 2883600 | tf_op jit(solution)/shard_map/all_gather | solution.py:55
  462.7 7.2 %convolution_convert_fusion = bf16[256,2048]{1,0:T(8,128)(2,1)S(1)} fusion(bf16[704,2048]{0,1:T(8,128)(2,1)} %all-gather.14.cloned.1.call-done, bf16[2048,1408]{1,0:T(8,128)(2,1)} %all-gather.12.cloned.1.call-done, f32[256,704]{0,1:T(8,128)S(1)} %fusion.2, f32[2048]{0:T(1024)S(1)} %bitcast.82, f32[256]{0:T(256)S(1)} %add_rsqrt_fusion.1, ...), kind=kOutput, calls=%fused_computation.12 | convolution fusion | flops 1480097792 | bytes 9118720 | tf_op jit(solution)/shard_map/dot_general | solution.py:188
  470.1 28.6 %all_to_all.31 = bf16[8,256,256]{2,1,0:T(8,128)(2,1)S(1)} all-to-all(bf16[8,256,256]{2,1,0:T(8,128)(2,1)S(1)} %bitcast.70), channel_id=1, replica_groups=mesh['fs_0'=16,'fs_1'=4,'tp'=8] {'tp'}, dimensions={0} | all-to-all | bytes 2097152 | tf_op jit(solution)/shard_map/all_to_all | solution.py:67
  499.5 4.3 all-to-all-start.3
  503.8 4.6 all-to-all-done.3
  (83 shorter events, 13.3 us)
Async XLA Ops:
  6.5 62.2 %copy-start.6 = (f32[2]{0:T(128)S(1)}, f32[2]{0:T(128)}, u32[]{:S(2)}) copy-start(f32[2]{0:T(128)} %param.24) | copy-start | bytes 28
  6.5 62.3 %all-gather.6.cloned.1.call-start = ((), (), s32[]{:S(2)}) async-start(), calls=%async_computation.4 | async-start | bytes 1216512 | tf_op jit(solution)/shard_map/all_gather | solution.py:20
  8.8 171.5 %all-gather.8.cloned.1.call-start = ((), (), s32[]{:S(2)}) async-start(), calls=%async_computation.5 | async-start | bytes 1597440 | tf_op jit(solution)/shard_map/all_gather | solution.py:31
  53.8 139.9 %all-to-all-start.1 = ((bf16[128,8,256]{2,0,1:T(8,128)(2,1)}), bf16[128,8,256]{2,0,1:T(8,128)(2,1)S(1)}, u32[]{:S(2)}, u32[]{:S(2)}) async-start(bf16[128,8,256]{2,0,1:T(8,128)(2,1)} %copy.31), calls=%async_computation.1 | async-start | bytes 1048576 | tf_op jit(solution)/shard_map/all_to_all | solution.py:173
  68.9 113.5 %copy-start = (bf16[2048,257]{0,1:T(8,128)(2,1)S(1)}, bf16[2048,257]{0,1:T(8,128)(2,1)}, u32[]{:S(2)}) copy-start(bf16[2048,257]{0,1:T(8,128)(2,1)} %all-gather.6.cloned.1.call-done) | copy-start | bytes 3158020
  192.1 17.6 %copy-start.7 = (bf16[256]{0:T(256)(128)(2,1)S(1)}, bf16[256]{0:T(256)(128)(2,1)}, u32[]{:S(2)}) copy-start(bf16[256]{0:T(256)(128)(2,1)} %param.25) | copy-start | bytes 1540
  193.7 25.8 %copy-start.2 = (bf16[256,256]{1,0:T(8,128)(2,1)S(1)}, bf16[256,256]{1,0:T(8,128)(2,1)}, u32[]{:S(2)}) copy-start(bf16[256,256]{1,0:T(8,128)(2,1)} %param.16) | copy-start | bytes 393220
  193.7 26.6 %copy-start.3 = (bf16[32,704]{1,0:T(8,128)(2,1)S(1)}, bf16[32,704]{1,0:T(8,128)(2,1)}, u32[]{:S(2)}) copy-start(bf16[32,704]{1,0:T(8,128)(2,1)} %param.27) | copy-start | bytes 135172
  193.7 26.6 %copy-start.4 = (bf16[32,704]{1,0:T(8,128)(2,1)S(1)}, bf16[32,704]{1,0:T(8,128)(2,1)}, u32[]{:S(2)}) copy-start(bf16[32,704]{1,0:T(8,128)(2,1)} %param.26) | copy-start | bytes 135172
  193.7 27.3 %copy-start.5 = (bf16[704,32]{0,1:T(8,128)(2,1)S(1)}, bf16[704,32]{0,1:T(8,128)(2,1)}, u32[]{:S(2)}) copy-start(bf16[704,32]{0,1:T(8,128)(2,1)} %param.28) | copy-start | bytes 135172
  194.6 24.4 %all-to-all-start = ((bf16[8,256,128]{2,1,0:T(8,128)(2,1)}), bf16[8,256,128]{2,1,0:T(8,128)(2,1)S(1)}, u32[]{:S(2)}, u32[]{:S(2)}) async-start(bf16[8,256,128]{2,1,0:T(8,128)(2,1)} %broadcast_in_dim.29), calls=%async_computation | async-start | bytes 1048576 | tf_op jit(solution)/shard_map/all_to_all | solution.py:43
  209.7 36.4 %all-gather.10.cloned.1.call-start = ((), (), s32[]{:S(2)}) async-start(), calls=%async_computation.6 | async-start | bytes 1216512 | tf_op jit(solution)/shard_map/all_gather | solution.py:20
  220.2 170.8 %all-gather.12.cloned.1.call-start = ((), (), s32[]{:S(2)}) async-start(), calls=%async_computation.7 | async-start | bytes 5857280 | tf_op jit(solution)/shard_map/all_gather | solution.py:31
  221.0 241.7 %all-gather.14.cloned.1.call-start = ((), (), s32[]{:S(2)}) async-start(), calls=%async_computation.8 | async-start | bytes 3342336 | tf_op jit(solution)/shard_map/all_gather | solution.py:55
  391.0 71.7 %copy-start.1 = (bf16[2048,257]{0,1:T(8,128)(2,1)S(1)}, bf16[2048,257]{0,1:T(8,128)(2,1)}, u32[]{:S(2)}) copy-start(bf16[2048,257]{0,1:T(8,128)(2,1)} %all-gather.10.cloned.1.call-done) | copy-start | bytes 3158020
  470.0 33.7 %copy-start.8 = (bf16[256]{0:T(256)(128)(2,1)S(1)}, bf16[256]{0:T(256)(128)(2,1)}, u32[]{:S(2)}) copy-start(bf16[256]{0:T(256)(128)(2,1)} %param.29) | copy-start | bytes 1540
  499.5 8.9 %all-to-all-start.3 = ((f32[8,256,1]{1,2,0:T(1,128)}), f32[8,256,1]{1,2,0:T(1,128)S(1)}, u32[]{:S(2)}, u32[]{:S(2)}) async-start(f32[8,256,1]{1,2,0:T(1,128)} %broadcast_in_dim.30), calls=%async_computation.3 | async-start | bytes 16384 | tf_op jit(solution)/shard_map/all_to_all | solution.py:43
Sparse Core Ops, SparseCore 0:
  9.4 36.6 all-gather.5
  49.1 131.1 all-gather.7
  220.3 25.6 all-gather.9
  248.8 142.1 all-gather.11
  392.9 69.7 all-gather.13
where the time goes:
time: 517 us; the launch traced here: 516 us
  waiting for transfers between devices  349 us (68%)
  blocking collectives  81 us (16%)
  starting transfers between devices  33.6 us (6%)
  matrix products  19.1 us (4%)
  between operations  14.1 us (3%)
  other arithmetic  12 us (2%)
  local copies, waits for them, and re-layouts  5.72 us (1%)
    all_gather x2, waiting for transfers between devices, sent_together(): filled = lax.all_gather(both, axis, axis=dim, tiled=True)  252 us
    all_gather x1, waiting for transfers between devices, gathered_by_axis(): filled = lax.all_gather(filled, axes[number], axis=dim, tiled=True)  68 us
    all_gather x3, blocking collectives, gathered_by_axis(): filled = lax.all_gather(filled, axes[number], axis=dim, tiled=True)  52.5 us
    all_to_all x1, blocking collectives, sent_and_summed(): tiles = lax.all_to_all(in_blocks(shard, dim, size), axis, 0, 0, tiled=True)  28.6 us
    all_to_all x2, starting transfers between devices, copy_for_each(): lax.all_to_all(jnp.broadcast_to(shard[None], (size, *shard.shape)), axis,...  19.4 us
    all_gather x2, waiting for transfers between devices, gather_turned(): filled, at, outs = (lax.all_gather(both, axis, axis=0, tiled=True), 0, [])  15 us
    all_to_all x1, starting transfers between devices, body(): lax.all_to_all(head_rows, 'tp', split_axis=1, concat_axis=0, tiled=True)  14.1 us
    all_to_all x2, waiting for transfers between devices, copy_for_each(): lax.all_to_all(jnp.broadcast_to(shard[None], (size, *shard.shape)), axis,...  14 us
  transfers between devices with their start and end apart: 8, of which 6 were waited for; matrix products, arithmetic and copies ran while one was open for 5% of the time, Pallas kernels for 0%

commit v1 on v0

--- a/solution.py
+++ b/solution.py
@@ -17,7 +17,13 @@
 def gather_turned(arrays, axis, dims):
     turned = [jnp.moveaxis(a, dim, 0) for a, dim in zip(arrays, dims)]
     both = jnp.concatenate([t.reshape(len(t), -1) for t in turned], axis=1)
-    filled, at, outs = (lax.all_gather(both, axis, axis=0, tiled=True), 0, [])
+    filled, at, outs = (
+        jnp.concatenate(
+            lax.all_to_all(jnp.stack([both] * lax.axis_size(axis)), axis, 0, 0), axis=0
+        ),
+        0,
+        [],
+    )
     for t, dim in zip(turned, dims):
         share = filled[:, at : at + t[0].size].reshape(-1, *t.shape[1:])
         outs.append(jnp.moveaxis(share, 0, dim))

time: 517 us -> 422 us (0.82)
  waiting for transfers between devices: 349 us -> 231 us
  blocking collectives: 81 us -> 96.1 us
  starting transfers between devices: 33.6 us -> 45.3 us
    all_gather x2, waiting for transfers between devices: 252 us -> 148 us  [sent_together(): filled = lax.all_gather(both, axis, axis=dim, tiled=True)]
    all_to_all x0 -> x1, blocking collectives: none -> 19.1 us  [gather_turned(): lax.all_to_all(jnp.stack([both] * lax.axis_size(axis)), axis, 0, 0)]
    all_gather x2 -> x0, waiting for transfers between devices: 15 us -> none  [gather_turned(): filled, at, outs = (lax.all_gather(both, axis, axis=0, tiled=True), 0, [])]
    all_to_all x0 -> x1, starting transfers between devices: none -> 10.4 us  [gather_turned(): lax.all_to_all(jnp.stack([both] * lax.axis_size(axis)), axis, 0, 0)]
  transfers between devices with their start and end apart: 8 -> 7, of which waited for: 6 -> 5; matrix products, arithmetic and copies ran while one was open for 5% -> 6% of each run, Pallas kernels for 0% -> 0%
where the time goes in v1:
time: 422 us; the launch traced here: 421 us
  waiting for transfers between devices  231 us (55%)
  blocking collectives  96.1 us (23%)
  starting transfers between devices  45.3 us (11%)
  matrix products  18.4 us (4%)
  between operations  14.1 us (3%)
  local copies, waits for them, and re-layouts  8.04 us (2%)
  other arithmetic  7.25 us (2%)
    all_gather x2, waiting for transfers between devices, sent_together(): filled = lax.all_gather(both, axis, axis=dim, tiled=True)  148 us
    all_gather x1, waiting for transfers between devices, gathered_by_axis(): filled = lax.all_gather(filled, axes[number], axis=dim, tiled=True)  68.6 us
    all_gather x3, blocking collectives, gathered_by_axis(): filled = lax.all_gather(filled, axes[number], axis=dim, tiled=True)  48.4 us
    all_to_all x1, blocking collectives, sent_and_summed(): tiles = lax.all_to_all(in_blocks(shard, dim, size), axis, 0, 0, tiled=True)  28.6 us
    all_to_all x2, starting transfers between devices, copy_for_each(): lax.all_to_all(jnp.broadcast_to(shard[None], (size, *shard.shape)), axis,...  19.4 us
    all_to_all x1, blocking collectives, gather_turned(): lax.all_to_all(jnp.stack([both] * lax.axis_size(axis)), axis, 0, 0)  19.1 us
    all_to_all x1, starting transfers between devices, body(): lax.all_to_all(head_rows, 'tp', split_axis=1, concat_axis=0, tiled=True)  15.5 us
    all_to_all x2, waiting for transfers between devices, copy_for_each(): lax.all_to_all(jnp.broadcast_to(shard[None], (size, *shard.shape)), axis,...  14 us
  transfers between devices with their start and end apart: 7, of which 5 were waited for; matrix products, arithmetic and copies ran while one was open for 6% of the time, Pallas kernels for 0%

profile of v1, /device:TPU:1, one launch (start us, length us, event | category | flops | bytes accessed | tf_op | source)
XLA Modules:
  0.0 421.4 jit_solution(10230742687199989510)
XLA Ops:
  6.5 1.4 pad_maximum_fusion.3
  8.1 1.5 pad_maximum_fusion.2
  11.2 1.1 stack.4
  12.3 10.4 %all-to-all-start = ((bf16[8,256,257]{1,2,0:T(8,128)(2,1)}), bf16[8,256,257]{1,2,0:T(8,128)(2,1)S(1)}, u32[]{:S(2)}, u32[]{:S(2)}) async-start(bf16[8,256,257]{1,2,0:T(8,128)(2,1)} %stack.4), calls=%async_computation | async-start | bytes 2162688 | tf_op jit(solution)/shard_map/all_to_all | solution.py:22
  22.7 10.5 %all_gather.22 = bf16[704,128]{0,1:T(8,128)(2,1)} all-gather(bf16[704,32]{0,1:T(8,128)(2,1)S(1)} %copy-done.1), channel_id=1, replica_groups=mesh['fs_0'=16,'fs_1'=4,'tp'=8] {'fs_1'}, dimensions={1}, use_global_device_ids=true | all-gather | bytes 225280 | tf_op jit(solution)/shard_map/all_gather | solution.py:61
  33.3 9.8 %all_gather.19 = bf16[128,128]{0,1:T(8,128)(2,1)S(1)} all-gather(bf16[128,32]{0,1:T(8,128)(2,1)S(1)} %copy-done.2), channel_id=1, replica_groups=mesh['fs_0'=16,'fs_1'=4,'tp'=8] {'fs_1'}, dimensions={1}, use_global_device_ids=true | all-gather | bytes 40960 | tf_op jit(solution)/shard_map/all_gather | solution.py:61
  43.1 28.1 %all_gather.20 = bf16[128,2048]{0,1:T(8,128)(2,1)S(1)} all-gather(bf16[128,128]{0,1:T(8,128)(2,1)S(1)} %all_gather.19), channel_id=1, replica_groups=mesh['fs_0'=16,'fs_1'=4,'tp'=8] {'fs_0'}, dimensions={1}, use_global_device_ids=true | all-gather | bytes 557056 | tf_op jit(solution)/shard_map/all_gather | solution.py:61
  73.0 15.5 %all-to-all-start.2 = ((bf16[128,8,256]{2,0,1:T(8,128)(2,1)}), bf16[128,8,256]{2,0,1:T(8,128)(2,1)S(1)}, u32[]{:S(2)}, u32[]{:S(2)}) async-start(bf16[128,8,256]{2,0,1:T(8,128)(2,1)} %copy.41), calls=%async_computation.2 | async-start | bytes 1048576 | tf_op jit(solution)/shard_map/all_to_all | solution.py:179
  89.4 56.7 %all-gather.4.cloned.1.call-done = bf16[2048,384]{1,0:T(8,128)(2,1)} async-done(((bf16[32,384]{1,0:T(8,128)(2,1)}), bf16[2048,384]{1,0:T(8,128)(2,1)}) %all-gather.4.cloned.1.call-update) | async-done | bytes 1572880 | tf_op jit(solution)/shard_map/all_gather | solution.py:37
  146.1 1.6 convolution_bitcast_fusion.1
  147.7 1.7 convolution_bitcast_fusion
  149.8 1.6 convolution_convert_fusion.2
  152.0 4.8 %while.13 = (s32[]{:T(128)}, f32[1,64,128]{2,1,0:T(8,128)S(1)}, f32[2,1,64,128]{3,2,1,0:T(8,128)S(1)}, f32[2]{0:T(128)S(1)}, f32[2,1]{0,1:T(1,128)S(1)}, /*index...) while((s32[]{:T(128)}, f32[1,64,128]{2,1,0:T(8,128)S(1)}, ...), condition=%wide.region_2.3_spmd.clone, body=%wide.region_1.2_spmd.clone.sunk | while | flops 49156 | bytes 164000 | solution.py:132
  157.4 1.6 fusion.35
  159.9 15.1 %all-to-all-start.1 = ((bf16[8,256,128]{2,1,0:T(8,128)(2,1)}), bf16[8,256,128]{2,1,0:T(8,128)(2,1)S(1)}, u32[]{:S(2)}, u32[]{:S(2)}) async-start(bf16[8,256,128]{2,1,0:T(8,128)(2,1)} %broadcast_in_dim.29), calls=%async_computation.1 | async-start | bytes 1048576 | tf_op jit(solution)/shard_map/all_to_all | solution.py:49
  175.0 9.3 %all-to-all-done.1 = bf16[8,256,128]{2,1,0:T(8,128)(2,1)S(1)} async-done(((bf16[8,256,128]{2,1,0:T(8,128)(2,1)}), bf16[8,256,128]{2,1,0:T(8,128)(2,1)S(1)}, u32[]{:S(2)}, u32[]{:S(2)}) %all-to-all-start.1) | async-done | bytes 524320 | tf_op jit(solution)/shard_map/all_to_all | solution.py:49
  184.9 19.1 %all_to_all.41 = bf16[8,256,257]{1,2,0:T(8,128)(2,1)S(1)} all-to-all(bf16[8,256,257]{1,2,0:T(8,128)(2,1)S(1)} %stack.5), channel_id=1, replica_groups=mesh['fs_0'=16,'fs_1'=4,'tp'=8] {'tp'}, dimensions={0} | all-to-all | bytes 2105344 | tf_op jit(solution)/shard_map/all_to_all | solution.py:22
  204.9 91.6 %all-gather.6.cloned.1.call-done = bf16[2048,1408]{1,0:T(8,128)(2,1)} async-done(((bf16[32,1408]{1,0:T(8,128)(2,1)}), bf16[2048,1408]{1,0:T(8,128)(2,1)}) %all-gather.6.cloned.1.call-update) | async-done | bytes 5767184 | tf_op jit(solution)/shard_map/all_gather | solution.py:37
  296.5 3.3 fusion.2
  299.8 68.6 %all-gather.8.cloned.1.call-done = bf16[704,2048]{0,1:T(8,128)(2,1)} async-done(((bf16[704,128]{0,1:T(8,128)(2,1)}), bf16[704,2048]{0,1:T(8,128)(2,1)}) %all-gather.8.cloned.1.call-update) | async-done | bytes 2883600 | tf_op jit(solution)/shard_map/all_gather | solution.py:61
  368.4 7.2 %convolution_convert_fusion = bf16[256,2048]{1,0:T(8,128)(2,1)S(1)} fusion(bf16[704,2048]{0,1:T(8,128)(2,1)} %all-gather.8.cloned.1.call-done, bf16[2048,1408]{1,0:T(8,128)(2,1)} %all-gather.6.cloned.1.call-done, f32[256,704]{0,1:T(8,128)S(1)} %fusion.2, f32[2048]{0:T(1024)S(1)} %bitcast.110, f32[256]{0:T(256)S(1)} %add_rsqrt_fusion.1, ...), kind=kOutput, calls=%fused_computation.12 | convolution fusion | flops 1480097792 | bytes 9118720 | tf_op jit(solution)/shard_map/dot_general | solution.py:194
  375.7 28.6 %all_to_all.42 = bf16[8,256,256]{2,1,0:T(8,128)(2,1)S(1)} all-to-all(bf16[8,256,256]{2,1,0:T(8,128)(2,1)S(1)} %bitcast.98), channel_id=1, replica_groups=mesh['fs_0'=16,'fs_1'=4,'tp'=8] {'tp'}, dimensions={0} | all-to-all | bytes 2097152 | tf_op jit(solution)/shard_map/all_to_all | solution.py:73
  405.1 4.3 %all-to-all-start.5 = ((f32[8,256,1]{1,2,0:T(1,128)}), f32[8,256,1]{1,2,0:T(1,128)S(1)}, u32[]{:S(2)}, u32[]{:S(2)}) async-start(f32[8,256,1]{1,2,0:T(1,128)} %broadcast_in_dim.30), calls=%async_computation.5 | async-start | bytes 16384 | tf_op jit(solution)/shard_map/all_to_all | solution.py:49
  409.4 4.6 %all-to-all-done.5 = f32[8,256,1]{1,2,0:T(1,128)S(1)} async-done(((f32[8,256,1]{1,2,0:T(1,128)}), f32[8,256,1]{1,2,0:T(1,128)S(1)}, u32[]{:S(2)}, u32[]{:S(2)}) %all-to-all-start.5) | async-done | bytes 8224 | tf_op jit(solution)/shard_map/all_to_all | solution.py:49
  (82 shorter events, 12.8 us)
Async XLA Ops:
  6.5 16.2 %copy-start.1 = (bf16[704,32]{0,1:T(8,128)(2,1)S(1)}, bf16[704,32]{0,1:T(8,128)(2,1)}, u32[]{:S(2)}) copy-start(bf16[704,32]{0,1:T(8,128)(2,1)} %param.28) | copy-start | bytes 135172
  6.5 139.6 %all-gather.4.cloned.1.call-start = ((), (), s32[]{:S(2)}) async-start(), calls=%async_computation.6 | async-start | bytes 1597440 | tf_op jit(solution)/shard_map/all_gather | solution.py:37
  8.0 288.5 %all-gather.6.cloned.1.call-start = ((), (), s32[]{:S(2)}) async-start(), calls=%async_computation.7 | async-start | bytes 5857280 | tf_op jit(solution)/shard_map/all_gather | solution.py:37
  9.6 23.7 %copy-start.2 = (bf16[128,32]{0,1:T(8,128)(2,1)S(1)}, bf16[128,32]{0,1:T(8,128)(2,1)}, u32[]{:S(2)}) copy-start(bf16[128,32]{0,1:T(8,128)(2,1)} %param.22) | copy-start | bytes 24580
  12.3 60.7 %copy-start.3 = (f32[2]{0:T(128)S(1)}, f32[2]{0:T(128)}, u32[]{:S(2)}) copy-start(f32[2]{0:T(128)} %param.24) | copy-start | bytes 28
  12.3 60.8 %all-to-all-start = ((bf16[8,256,257]{1,2,0:T(8,128)(2,1)}), bf16[8,256,257]{1,2,0:T(8,128)(2,1)S(1)}, u32[]{:S(2)}, u32[]{:S(2)}) async-start(bf16[8,256,257]{1,2,0:T(8,128)(2,1)} %stack.4), calls=%async_computation | async-start | bytes 2162688 | tf_op jit(solution)/shard_map/all_to_all | solution.py:22
  22.7 345.7 %all-gather.8.cloned.1.call-start = ((), (), s32[]{:S(2)}) async-start(), calls=%async_computation.8 | async-start | bytes 3342336 | tf_op jit(solution)/shard_map/all_gather | solution.py:61
  73.0 86.0 %all-to-all-start.2 = ((bf16[128,8,256]{2,0,1:T(8,128)(2,1)}), bf16[128,8,256]{2,0,1:T(8,128)(2,1)S(1)}, u32[]{:S(2)}, u32[]{:S(2)}) async-start(bf16[128,8,256]{2,0,1:T(8,128)(2,1)} %copy.41), calls=%async_computation.2 | async-start | bytes 1048576 | tf_op jit(solution)/shard_map/all_to_all | solution.py:179
  157.4 17.6 %copy-start.4 = (bf16[256]{0:T(256)(128)(2,1)S(1)}, bf16[256]{0:T(256)(128)(2,1)}, u32[]{:S(2)}) copy-start(bf16[256]{0:T(256)(128)(2,1)} %param.25) | copy-start | bytes 1540
  159.0 25.8 %copy-start = (bf16[256,256]{1,0:T(8,128)(2,1)S(1)}, bf16[256,256]{1,0:T(8,128)(2,1)}, u32[]{:S(2)}) copy-start(bf16[256,256]{1,0:T(8,128)(2,1)} %param.16) | copy-start | bytes 393220
  159.9 24.4 %all-to-all-start.1 = ((bf16[8,256,128]{2,1,0:T(8,128)(2,1)}), bf16[8,256,128]{2,1,0:T(8,128)(2,1)S(1)}, u32[]{:S(2)}, u32[]{:S(2)}) async-start(bf16[8,256,128]{2,1,0:T(8,128)(2,1)} %broadcast_in_dim.29), calls=%async_computation.1 | async-start | bytes 1048576 | tf_op jit(solution)/shard_map/all_to_all | solution.py:49
  375.7 33.7 %copy-start.5 = (bf16[256]{0:T(256)(128)(2,1)S(1)}, bf16[256]{0:T(256)(128)(2,1)}, u32[]{:S(2)}) copy-start(bf16[256]{0:T(256)(128)(2,1)} %param.29) | copy-start | bytes 1540
  405.1 8.9 %all-to-all-start.5 = ((f32[8,256,1]{1,2,0:T(1,128)}), f32[8,256,1]{1,2,0:T(1,128)S(1)}, u32[]{:S(2)}, u32[]{:S(2)}) async-start(f32[8,256,1]{1,2,0:T(1,128)} %broadcast_in_dim.30), calls=%async_computation.5 | async-start | bytes 16384 | tf_op jit(solution)/shard_map/all_to_all | solution.py:49
Sparse Core Ops, SparseCore 0:
  10.3 135.7 all-gather.3
  149.0 147.4 all-gather.5
  298.6 69.7 all-gather.7
